TPU v7x, 32 devices: a whole 2x2x4 slice. The times are simulated.
32 devices in a mesh: grp: 2 (over y), fs: 4 (over z), tp: 4 (over x, core).
Axes of the slice: x: 2, y: 2, z: 4, core: 2. Of those that a mesh axis runs over, the one named last changes fastest.
Arguments:
- tokens: bfloat16 [4096, 2048], P(('grp', 'fs')), parts along dimension 0, may hold values from -6 to 6
- norm_gain: float32 [2, 2048], replicated, may hold values from 0.1 to 1.9
- norm_shift: float32 [2, 2048], replicated, may hold values from -3 to 3
- gate_first: bfloat16 [2048, 3072], P('fs', 'tp'), may hold values from -0.125 to 0.125
- up_first: bfloat16 [2048, 3072], P('fs', 'tp'), may hold values from -0.125 to 0.125
- down_first: bfloat16 [3072, 2048], P('tp', 'fs'), may hold values from -0.21875 to 0.21875
- gate_second: bfloat16 [2048, 3072], P('fs', 'tp'), may hold values from -0.125 to 0.125
- up_second: bfloat16 [2048, 3072], P('fs', 'tp'), may hold values from -0.125 to 0.125
- down_second: bfloat16 [3072, 2048], P('tp', 'fs'), may hold values from -0.21875 to 0.21875
Outputs:
- encoded: bfloat16 [4096, 2048], P(('grp', 'fs')), parts along dimension 0
There are 2 independent parts, one for each index of `grp`. A program takes and returns all parts, laid end to end along the dimension named above; an argument that names none is the same for every part. Nothing has to cross between parts.
All inputs are finite; a program needn't handle non-finite values.
Results may differ from a plain program's by a relative error of at most 0.012.
Values may be sent and summed in bfloat16 or wider, within the bound.
A program may use at most 64 MiB of HBM per device.

v0:
```python
import jax
import jax.numpy as jnp
from jax import lax
from jax.sharding import PartitionSpec as P


def post_norm(values, gain, shift):
    mean = jnp.mean(values, axis=-1, keepdims=True)
    spread = jnp.mean(jnp.square(values - mean), axis=-1, keepdims=True)
    normed = (values - mean) * lax.rsqrt(spread + 1e-05)
    return (normed * gain + shift).astype(jnp.bfloat16)


def rounded_term(stream_rows, down_full):
    return jnp.dot(stream_rows, down_full, preferred_element_type=jnp.float32).astype(jnp.bfloat16)


def half_step(stream, gate_w, up_w, down_w, gain, shift):
    width = gate_w.shape[1]
    joined = jnp.concatenate(
        (
            lax.all_gather(gate_w, "fs", axis=0, tiled=True),
            lax.all_gather(up_w, "fs", axis=0, tiled=True),
        ),
        axis=1,
    )
    both = jnp.dot(stream, joined, preferred_element_type=jnp.float32)
    gate = both[:, :width]
    up = both[:, width:]
    hidden = (jax.nn.silu(gate) * up).astype(jnp.bfloat16)
    scale = 2.0**0.25
    down_full = lax.all_gather(down_w, "fs", axis=1, tiled=True)
    partial_value = rounded_term(hidden, down_full)
    branch = lax.psum(partial_value, "tp").astype(jnp.float32).astype(jnp.bfloat16)
    return post_norm(
        scale * stream.astype(jnp.float32) + 0.5 * branch.astype(jnp.float32), gain, shift
    )


def local(
    tokens,
    norm_gain,
    norm_shift,
    gate_first,
    up_first,
    down_first,
    gate_second,
    up_second,
    down_second,
):
    middle = half_step(tokens, gate_first, up_first, down_first, norm_gain[0], norm_shift[0])
    return half_step(middle, gate_second, up_second, down_second, norm_gain[1], norm_shift[1])


def solution(mesh):
    placed = (
        P(("grp", "fs"), None),
        P(),
        P(),
        P("fs", "tp"),
        P("fs", "tp"),
        P("tp", "fs"),
        P("fs", "tp"),
        P("fs", "tp"),
        P("tp", "fs"),
    )
    return jax.shard_map(
        local, mesh=mesh, in_specs=placed, out_specs=P(("grp", "fs"), None), check_vma=False
    )
```

profile of v0, /device:TPU:0, one launch (start us, length us, event | category | flops | bytes accessed | tf_op | source)
XLA Modules:
  0.0 519.6 jit_solution(14808185520538437367)
XLA Ops:
  6.5 0.0 all-gather.7.cloned.1.call-start
  6.5 0.7 all-gather.7.cloned.1.call-update
  7.3 0.0 all-gather.9.cloned.1.call-start
  7.3 0.7 all-gather.9.cloned.1.call-update
  8.0 0.0 all-gather.11.cloned.1.call-start
  8.1 0.7 all-gather.11.cloned.1.call-update
  8.7 0.0 all-reduce.3.cloned.1.call-start
  8.8 66.3 %all-gather.7.cloned.1.call-done = bf16[2048,768]{1,0:T(8,128)(2,1)} async-done(((bf16[512,768]{1,0:T(8,128)(2,1)}), bf16[2048,768]{1,0:T(8,128)(2,1)}) %all-gather.7.cloned.1.call-update) | async-done | bytes 3145744 | tf_op jit(solution)/shard_map/all_gather | solution.py:22
  75.1 63.7 %all-gather.9.cloned.1.call-done = bf16[2048,768]{1,0:T(8,128)(2,1)} async-done(((bf16[512,768]{1,0:T(8,128)(2,1)}), bf16[2048,768]{1,0:T(8,128)(2,1)}) %all-gather.9.cloned.1.call-update) | async-done | bytes 3145744 | tf_op jit(solution)/shard_map/all_gather | solution.py:23
  138.8 6.9 %fusion.8 = f32[512,1536]{0,1:T(8,128)S(1)} fusion(bf16[512,2048]{1,0:T(8,128)(2,1)} %param.9, bf16[2048,768]{1,0:T(8,128)(2,1)} %all-gather.9.cloned.1.call-done, bf16[2048,768]{1,0:T(8,128)(2,1)} %all-gather.7.cloned.1.call-done), kind=kOutput, calls=%fused_computation.14 | convolution fusion | flops 3233808384 | bytes 11534336 | tf_op jit(solution)/shard_map/dot_general | solution.py:27
  145.7 56.7 %all-gather.11.cloned.1.call-done = bf16[768,2048]{1,0:T(8,128)(2,1)} async-done(((bf16[768,512]{1,0:T(8,128)(2,1)}), bf16[768,2048]{1,0:T(8,128)(2,1)}) %all-gather.11.cloned.1.call-update) | async-done | bytes 3145744 | tf_op jit(solution)/shard_map/all_gather | solution.py:32
  202.5 5.1 convolution_convert_fusion.1
  207.6 0.0 copy-start.4
  207.6 0.0 copy-start.5
  207.6 0.0 copy-start
  207.6 0.0 all-reduce.3.cloned.1.call-update
  207.6 0.0 all-gather.13.cloned.1.call-start
  207.7 0.5 all-gather.13.cloned.1.call-update
  208.2 0.0 all-gather.15.cloned.1.call-start
  208.3 0.5 all-gather.15.cloned.1.call-update
  208.8 0.0 all-gather.17.cloned.1.call-start
  208.8 0.7 all-gather.17.cloned.1.call-update
  209.5 0.2 all-reduce.5.cloned.1.call-start
  209.8 0.0 copy-done.4
  209.8 0.0 copy-done.5
  209.8 48.0 %all-reduce.3.cloned.1.call-done = bf16[512,2048]{1,0:T(8,128)(2,1)} async-done(((bf16[512,2048]{1,0:T(8,128)(2,1)}), bf16[512,2048]{1,0:T(8,128)(2,1)}) %all-reduce.3.cloned.1.call-update) | async-done | bytes 2097168 | tf_op jit(solution)/shard_map/psum | solution.py:34
  257.8 0.0 copy-done
  257.8 0.0 copy-start.2
  257.8 2.6 fusion.11
  260.4 0.0 copy-start.1
  260.4 0.0 copy-done.2
  260.5 1.2 multiply_reduce_fusion.1
  261.6 0.4 copy-done.1
  262.0 1.3 add_convert_fusion.1
  263.4 59.4 %all-gather.13.cloned.1.call-done = bf16[2048,768]{1,0:T(8,128)(2,1)} async-done(((bf16[512,768]{1,0:T(8,128)(2,1)}), bf16[2048,768]{1,0:T(8,128)(2,1)}) %all-gather.13.cloned.1.call-update) | async-done | bytes 3145744 | tf_op jit(solution)/shard_map/all_gather | solution.py:22
  322.8 63.5 %all-gather.15.cloned.1.call-done = bf16[2048,768]{1,0:T(8,128)(2,1)} async-done(((bf16[512,768]{1,0:T(8,128)(2,1)}), bf16[2048,768]{1,0:T(8,128)(2,1)}) %all-gather.15.cloned.1.call-update) | async-done | bytes 3145744 | tf_op jit(solution)/shard_map/all_gather | solution.py:23
  386.3 8.0 %fusion.4 = f32[512,1536]{0,1:T(8,128)} fusion(bf16[512,2048]{1,0:T(8,128)(2,1)S(1)} %add_convert_fusion.1, bf16[2048,768]{1,0:T(8,128)(2,1)} %all-gather.15.cloned.1.call-done, bf16[2048,768]{1,0:T(8,128)(2,1)} %all-gather.13.cloned.1.call-done), kind=kOutput, calls=%fused_computation.4 | convolution fusion | flops 3233808384 | bytes 11534336 | tf_op jit(solution)/shard_map/dot_general | solution.py:27
  394.3 55.7 %all-gather.17.cloned.1.call-done = bf16[768,2048]{1,0:T(8,128)(2,1)} async-done(((bf16[768,512]{1,0:T(8,128)(2,1)}), bf16[768,2048]{1,0:T(8,128)(2,1)}) %all-gather.17.cloned.1.call-update) | async-done | bytes 3145744 | tf_op jit(solution)/shard_map/all_gather | solution.py:32
  450.0 6.1 %convolution_convert_fusion = bf16[512,2048]{1,0:T(8,128)(2,1)} fusion(bf16[768,2048]{1,0:T(8,128)(2,1)} %all-gather.17.cloned.1.call-done, f32[512,1536]{0,1:T(8,128)} %fusion.4), kind=kOutput, calls=%fused_computation.15 | convolution fusion | flops 1614020608 | bytes 8388608 | tf_op jit(solution)/shard_map/dot_general | solution.py:15
  456.1 0.0 all-reduce.5.cloned.1.call-update
  456.1 50.2 %all-reduce.5.cloned.1.call-done = bf16[512,2048]{1,0:T(8,128)(2,1)} async-done(((bf16[512,2048]{1,0:T(8,128)(2,1)}), bf16[512,2048]{1,0:T(8,128)(2,1)}) %all-reduce.5.cloned.1.call-update) | async-done | bytes 2097168 | tf_op jit(solution)/shard_map/psum | solution.py:34
  506.3 0.0 copy-start.3
  506.3 2.6 fusion.12
  508.9 0.0 copy-done.3
  508.9 1.2 multiply_reduce_fusion
  510.1 2.6 add_convert_fusion
  (6 shorter events, 0.1 us)
Async XLA Ops:
  6.5 68.6 %all-gather.7.cloned.1.call-start = ((), (), s32[]{:S(2)}) async-start(), calls=%async_computation | async-start | bytes 3932160 | tf_op jit(solution)/shard_map/all_gather | solution.py:22
  7.3 131.5 %all-gather.9.cloned.1.call-start = ((), (), s32[]{:S(2)}) async-start(), calls=%async_computation.1 | async-start | bytes 3932160 | tf_op jit(solution)/shard_map/all_gather | solution.py:23
  8.0 194.5 %all-gather.11.cloned.1.call-start = ((), (), s32[]{:S(2)}) async-start(), calls=%async_computation.2 | async-start | bytes 3932160 | tf_op jit(solution)/shard_map/all_gather | solution.py:32
  8.7 249.1 %all-reduce.3.cloned.1.call-start = ((), (), s32[]{:S(2)}) async-start(), calls=%async_computation.3 | async-start | bytes 4194304 | tf_op jit(solution)/shard_map/psum | solution.py:34
  207.6 2.2 copy-start.4
  207.6 2.2 copy-start.5
  207.6 50.2 %copy-start = (bf16[512,2048]{1,0:T(8,128)(2,1)S(1)}, bf16[512,2048]{1,0:T(8,128)(2,1)}, u32[]{:S(2)}) copy-start(bf16[512,2048]{1,0:T(8,128)(2,1)} %param.9) | copy-start | bytes 6291460
  207.6 115.1 %all-gather.13.cloned.1.call-start = ((), (), s32[]{:S(2)}) async-start(), calls=%async_computation.4 | async-start | bytes 3932160 | tf_op jit(solution)/shard_map/all_gather | solution.py:22
  208.2 178.1 %all-gather.15.cloned.1.call-start = ((), (), s32[]{:S(2)}) async-start(), calls=%async_computation.5 | async-start | bytes 3932160 | tf_op jit(solution)/shard_map/all_gather | solution.py:23
  208.8 241.2 %all-gather.17.cloned.1.call-start = ((), (), s32[]{:S(2)}) async-start(), calls=%async_computation.6 | async-start | bytes 3932160 | tf_op jit(solution)/shard_map/all_gather | solution.py:32
  209.5 296.7 %all-reduce.5.cloned.1.call-start = ((), (), s32[]{:S(2)}) async-start(), calls=%async_computation.7 | async-start | bytes 4194304 | tf_op jit(solution)/shard_map/psum | solution.py:34
  257.8 2.6 copy-start.2
  260.4 1.6 copy-start.1
  506.3 2.6 copy-start.3
Sparse Core Ops, SparseCore 0:
  8.9 66.1 all-gather.6
  76.7 62.0 all-gather.8
  140.4 62.0 all-gather.10
  207.7 50.0 all-reduce.2
  259.2 63.5 all-gather.12
  324.2 62.0 all-gather.14
  387.9 62.0 all-gather.16
  456.2 49.9 all-reduce.4
where the time goes:
time: 520 us
  waiting for transfers between devices  467 us (90%)
  matrix products  26.1 us (5%)
  between operations  13.6 us (3%)
  other arithmetic  11.6 us (2%)
    all_gather x2, waiting for transfers between devices, half_step(): lax.all_gather(up_w, 'fs', axis=0, tiled=True)  127 us
    all_gather x2, waiting for transfers between devices, half_step(): lax.all_gather(gate_w, 'fs', axis=0, tiled=True)  126 us
    all_gather x2, waiting for transfers between devices, half_step(): down_full = lax.all_gather(down_w, 'fs', axis=1, tiled=True)  112 us
    psum x2, waiting for transfers between devices, half_step(): lax.psum(partial_value, 'tp').astype(jnp.float32).astype(jnp.bfloat16)  98.1 us
    dot_general x2, matrix products, half_step(): both = jnp.dot(stream, joined, preferred_element_type=jnp.float32)  14.9 us
    dot_general x2, matrix products, rounded_term(): jnp.dot(stream_rows, down_full, preferred_element_type=jnp.float32)  11.2 us
  transfers between devices with their start and end apart: 8, of which 8 were waited for; matrix products, arithmetic and copies ran while one was open for 4% of the time, Pallas kernels for 0%

commit v1 on v0

--- a/solution.py
+++ b/solution.py
@@ -1,7 +1,317 @@
+import functools
+
 import jax
 import jax.numpy as jnp
 from jax import lax
+from jax.experimental import pallas as pl
+from jax.experimental.pallas import tpu as pltpu
 from jax.sharding import PartitionSpec as P
+
+MESH = pl.DeviceIdType.MESH
+SCALE = 2.0**0.25
+F32 = jnp.float32
+BF16 = jnp.bfloat16
+
+
+def aligned(value, step):
+    return pl.multiple_of(value, step)
+
+
+def fused_kernel(nf, nt, *refs):
+    tokens, gains, shifts = refs[:3]
+    shards = refs[3:9]
+    out = refs[9]
+    full = refs[10:16]
+    gate, hidden, part, middle, pair, ring = refs[16:22]
+    z_recv, y_recv, right_sent, left_sent, y_sent, own_done = refs[22:28]
+    core_sent, core_recv, x_sent, x_recv, swap_sent, swap_recv = refs[28:34]
+
+    g = lax.axis_index("grp")
+    f = lax.axis_index("fs")
+    t = lax.axis_index("tp")
+    other_g = 1 - g
+    chip, core = t // 2, t % 2
+    chips = nt // 2
+    peer = chip * 2 + (1 - core)
+    rows, width = tokens.shape
+    half = rows // 2
+    depth = width // nf
+
+    def tell(**where):
+        pl.semaphore_signal(barrier, inc=1, device_id=where, device_id_type=MESH)
+
+    barrier = pltpu.get_barrier_semaphore()
+    pl.when(f > 0)(lambda: tell(fs=f - 1))
+    pl.when(f < nf - 1)(lambda: tell(fs=f + 1))
+    tell(grp=other_g)
+    tell(tp=peer)
+    for step in range(1, chips):
+        tell(tp=lax.rem(chip + step, chips) * 2 + core)
+    ends = jnp.where(f > 0, 1, 0) + jnp.where(f < nf - 1, 1, 0)
+    pl.semaphore_wait(barrier, ends + 1 + chips)
+
+    def shard_part(a, which):
+        size = shards[a].shape[0] // 2
+        return shards[a].at[pl.ds(aligned(which * size, size), size), :]
+
+    def slot(a, s, which):
+        if a % 3 == 2:
+            size = full[a].shape[1] // 2
+            return full[a].at[s, pl.ds(aligned(which * size, size), size), :]
+        size = depth // 2
+        return full[a].at[pl.ds(aligned(s * depth + which * size, size), size), :]
+
+    def whole_slot(a, s):
+        if a % 3 == 2:
+            return full[a].at[s]
+        return full[a].at[pl.ds(aligned(s * depth, depth), depth), :]
+
+    def own(a):
+        return pltpu.make_async_copy(shards[a], whole_slot(a, f), own_done.at[a])
+
+    def to_right(a, s, src):
+        return pltpu.make_async_remote_copy(
+            src, slot(a, s, g), right_sent.at[a, s], z_recv.at[a, s],
+            device_id={"fs": f + 1}, device_id_type=MESH)
+
+    def to_left(a, s, src):
+        return pltpu.make_async_remote_copy(
+            src, slot(a, s, g), left_sent.at[a, s], z_recv.at[a, s],
+            device_id={"fs": f - 1}, device_id_type=MESH)
+
+    def across(a, s, which):
+        return pltpu.make_async_remote_copy(
+            slot(a, s, which), slot(a, s, which), y_sent.at[a, s], y_recv.at[a, s],
+            device_id={"grp": other_g}, device_id_type=MESH)
+
+    def send_own(a):
+        pl.when(f < nf - 1)(lambda: to_right(a, f, shard_part(a, g)).start())
+        pl.when(f > 0)(lambda: to_left(a, f, shard_part(a, g)).start())
+
+    def hop(a, h):
+        @pl.when(f - h >= 0)
+        def _():
+            s = f - h
+            to_left(a, s, slot(a, s, g)).wait_recv()
+            pl.when(f < nf - 1)(lambda: to_right(a, s, slot(a, s, g)).start())
+            across(a, s, g).start()
+
+        @pl.when(f + h < nf)
+        def _():
+            s = f + h
+            to_right(a, s, slot(a, s, g)).wait_recv()
+            pl.when(f > 0)(lambda: to_left(a, s, slot(a, s, g)).start())
+            across(a, s, g).start()
+
+    def at_distance(h, work):
+        if h == 0:
+            work(f)
+            return
+        pl.when(f - h >= 0)(lambda: work(f - h))
+        pl.when(f + h < nf)(lambda: work(f + h))
+
+    def crossed(a, s):
+        across(a, s, other_g).wait_recv()
+
+    def arrived(a):
+        own(a).wait()
+        for h in range(1, nf):
+            at_distance(h, lambda s: crossed(a, s))
+
+    tile = 256 if gate.shape[1] % 256 == 0 else gate.shape[1]
+
+    def project_gate(a, stream):
+        @pl.loop(0, gate.shape[1] // tile)
+        def _(i):
+            cols = pl.ds(aligned(i * tile, tile), tile)
+            gate[:, cols] = jnp.dot(stream[...], full[a][:, cols], preferred_element_type=F32)
+
+    def project_up(a, stream):
+        @pl.loop(0, gate.shape[1] // tile)
+        def _(i):
+            cols = pl.ds(aligned(i * tile, tile), tile)
+            up = jnp.dot(stream[...], full[a][:, cols], preferred_element_type=F32)
+            hidden[:, cols] = (jax.nn.silu(gate[:, cols]) * up).astype(BF16)
+
+    def columns(s):
+        return pl.ds(aligned(s * depth, depth), depth)
+
+    mine = pl.ds(aligned(core * half, half), half)
+    theirs = pl.ds(aligned((1 - core) * half, half), half)
+
+    def core_copy(layer, s):
+        return pltpu.make_async_remote_copy(
+            part.at[layer, theirs, columns(s)], pair.at[layer, :, columns(s)],
+            core_sent.at[layer, s], core_recv.at[layer, s],
+            device_id={"tp": peer}, device_id_type=MESH)
+
+    def x_copy(layer, s, source, target):
+        return pltpu.make_async_remote_copy(
+            ring.at[layer, source, :, columns(s)], ring.at[layer, source, :, columns(s)],
+            x_sent.at[layer, s, target], x_recv.at[layer, s, source],
+            device_id={"tp": target * 2 + core}, device_id_type=MESH)
+
+    def partial(layer, s):
+        part[layer, :, columns(s)] = jnp.dot(
+            hidden[...], full[3 * layer + 2][s], preferred_element_type=F32).astype(BF16)
+        core_copy(layer, s).start()
+
+    def pair_sum(layer, s):
+        core_copy(layer, s).wait_recv()
+        ring[layer, chip, :, columns(s)] = (
+            part[layer, mine, columns(s)].astype(F32) + pair[layer, :, columns(s)].astype(F32)
+        ).astype(BF16)
+        for step in range(1, chips):
+            x_copy(layer, s, chip, lax.rem(chip + step, chips)).start()
+
+    def chips_in(layer, s):
+        for step in range(1, chips):
+            source = lax.rem(chip + step, chips)
+            x_copy(layer, s, source, source).wait_recv()
+
+    def swap_copy(layer, target):
+        return pltpu.make_async_remote_copy(
+            target.at[mine, :], target.at[mine, :], swap_sent.at[layer], swap_recv.at[layer],
+            device_id={"tp": peer}, device_id_type=MESH)
+
+    def swap_in(layer, target):
+        return pltpu.make_async_remote_copy(
+            target.at[theirs, :], target.at[theirs, :], swap_sent.at[layer], swap_recv.at[layer],
+            device_id={"tp": peer}, device_id_type=MESH)
+
+    def norm(layer, stream, target):
+        band = 32
+
+        @pl.loop(0, half // band)
+        def _(i):
+            here = pl.ds(aligned(i * band, band), band)
+            there = pl.ds(aligned(core * half + i * band, band), band)
+            total = ring[layer, 0, here, :].astype(F32)
+            for c in range(1, chips):
+                total = total + ring[layer, c, here, :].astype(F32)
+            branch = total.astype(BF16).astype(F32)
+            v = SCALE * stream[there, :].astype(F32) + 0.5 * branch
+            mean = jnp.mean(v, axis=-1, keepdims=True)
+            v = v - mean
+            spread = jnp.mean(v * v, axis=-1, keepdims=True)
+            normed = v * lax.rsqrt(spread + 1e-05)
+            target[there, :] = (
+                normed * gains[layer:layer + 1, :] + shifts[layer:layer + 1, :]).astype(BF16)
+
+        swap_copy(layer, target).start()
+        swap_in(layer, target).wait_recv()
+
+    def all_shards(work):
+        for h in range(nf):
+            at_distance(h, work)
+
+    for a in range(2):
+        send_own(a)
+    for a in range(6):
+        own(a).start()
+
+    for a in range(5):
+        if a > 0:
+            send_own(a + 1)
+        hop(a, 1)
+        if a == 1:
+            arrived(0)
+            project_gate(0, tokens)
+        if a == 2:
+            arrived(1)
+            project_up(1, tokens)
+        if a == 3:
+            arrived(2)
+
+            @pl.loop(0, nf)
+            def _(s):
+                partial(0, s)
+
+            @pl.loop(0, nf)
+            def _(s):
+                pair_sum(0, s)
+
+        if a == 4:
+            @pl.loop(0, nf)
+            def _(s):
+                chips_in(0, s)
+
+            norm(0, tokens, middle)
+            arrived(3)
+            project_gate(3, middle)
+        for h in range(2, nf):
+            hop(a, h)
+
+    hop(5, 1)
+    arrived(4)
+    project_up(4, middle)
+    own(5).wait()
+    partial(1, f)
+    for h in range(2, nf + 1):
+        if h < nf:
+            hop(5, h)
+
+        def finish(s):
+            crossed(5, s)
+            partial(1, s)
+
+        at_distance(h - 2, lambda s: pair_sum(1, s))
+        at_distance(h - 1, finish)
+    at_distance(nf - 1, lambda s: pair_sum(1, s))
+
+    @pl.loop(0, nf)
+    def _(s):
+        chips_in(1, s)
+
+    norm(1, middle, out)
+
+    for a in range(6):
+        @pl.loop(0, nf)
+        def _(s):
+            pl.when((s <= f) & (f < nf - 1))(lambda: to_right(a, s, slot(a, s, g)).wait_send())
+            pl.when((s >= f) & (f > 0))(lambda: to_left(a, s, slot(a, s, g)).wait_send())
+            pl.when(s != f)(lambda: across(a, s, g).wait_send())
+
+    for layer in range(2):
+        @pl.loop(0, nf)
+        def _(s):
+            core_copy(layer, s).wait_send()
+            for step in range(1, chips):
+                x_copy(layer, s, chip, lax.rem(chip + step, chips)).wait_send()
+
+    swap_copy(0, middle).wait_send()
+    swap_copy(1, out).wait_send()
+
+
+def fused(nf, nt, tokens, gains, shifts, *weights):
+    rows, width = tokens.shape
+    units = weights[0].shape[1]
+    depth = width // nf
+    side = pltpu.VMEM((width, units), BF16)
+    down = pltpu.VMEM((nf, units, depth), BF16)
+    dma = pltpu.SemaphoreType.DMA
+    chips = nt // 2
+    return pl.pallas_call(
+        functools.partial(fused_kernel, nf, nt),
+        out_shape=jax.ShapeDtypeStruct((rows, width), BF16),
+        in_specs=[pl.BlockSpec(memory_space=pltpu.VMEM)] * 3
+        + [pl.BlockSpec(memory_space=pl.ANY)] * 6,
+        out_specs=pl.BlockSpec(memory_space=pltpu.VMEM),
+        scratch_shapes=[
+            side, side, down, side, side, down,
+            pltpu.VMEM((rows, units), F32),
+            pltpu.VMEM((rows, units), BF16),
+            pltpu.VMEM((2, rows, width), BF16),
+            pltpu.VMEM((rows, width), BF16),
+            pltpu.VMEM((2, rows // 2, width), BF16),
+            pltpu.VMEM((2, chips, rows // 2, width), BF16),
+            dma((6, nf)), dma((6, nf)), dma((6, nf)), dma((6, nf)), dma((6, nf)), dma((6,)),
+            dma((2, nf)), dma((2, nf)), dma((2, nf, chips)), dma((2, nf, chips)),
+            dma((2,)), dma((2,)),
+        ],
+        compiler_params=pltpu.CompilerParams(
+            collective_id=0, has_side_effects=True, vmem_limit_bytes=60 * 1024 * 1024),
+    )(tokens, gains, shifts, *weights)
 
 
 def post_norm(values, gain, shift):
@@ -52,7 +362,22 @@
     return half_step(middle, gate_second, up_second, down_second, norm_gain[1], norm_shift[1])
 
 
+def fits(mesh, args):
+    tokens, gate_first = args[0], args[3]
+    nf, nt = mesh.shape["fs"], mesh.shape["tp"]
+    depth, units = gate_first.shape
+    return (
+        mesh.shape["grp"] == 2 and nt % 2 == 0 and 1 < nf <= 8
+        and depth % 128 == 0 and units % 128 == 0 and tokens.shape[0] % 64 == 0
+    )
+
+
 def solution(mesh):
+    def either(*args):
+        if fits(mesh, args):
+            return fused(mesh.shape["fs"], mesh.shape["tp"], *args)
+        return local(*args)
+
     placed = (
         P(("grp", "fs"), None),
         P(),
@@ -65,5 +390,5 @@
         P("tp", "fs"),
     )
     return jax.shard_map(
-        local, mesh=mesh, in_specs=placed, out_specs=P(("grp", "fs"), None), check_vma=False
-    )
+        either, mesh=mesh, in_specs=placed, out_specs=P(("grp", "fs"), None), check_vma=False
+    )

time: 520 us -> 203 us (0.39)
  waiting for transfers between devices: 467 us -> 0 us
  Pallas kernels: 0 us -> 199 us
  matrix products: 26.1 us -> 0 us
  between operations: 13.6 us -> 0.01 us
  other arithmetic: 11.6 us -> 0 us
    all_gather x6 -> x0, waiting for transfers between devices: 365 us -> none  [the longest x2 127 us: half_step(): lax.all_gather(up_w, 'fs', axis=0, tiled=True)]
    pallas_call x0 -> x1, Pallas kernels: none -> 199 us  [fused(): pl.pallas_call(functools.partial(fused_kernel, nf, nt), out_shape=jax.Sha...]
    psum x2 -> x0, waiting for transfers between devices: 98.1 us -> none  [half_step(): lax.psum(partial_value, 'tp').astype(jnp.float32).astype(jnp.bfloat16)]
    dot_general x4 -> x0, matrix products: 26.1 us -> none  [the longest x2 14.9 us: half_step(): both = jnp.dot(stream, joined, preferred_element_type=jnp.float32)]
    reduce_sum x4 -> x0, other arithmetic: 7.58 us -> none  [the longest x2 5.25 us: post_norm(): mean = jnp.mean(values, axis=-1, keepdims=True)]
  transfers between devices with their start and end apart: 8 -> 0, of which waited for: 8 -> 0; matrix products, arithmetic and copies ran while one was open for 4% -> 0% of each run, Pallas kernels for 0% -> 0%
where the time goes in v1:
time: 203 us; the launch traced here: 202 us
  Pallas kernels  199 us (98%)
  local copies, waits for them, and re-layouts  3.16 us (2%)
    pallas_call x1, Pallas kernels, fused(): pl.pallas_call(functools.partial(fused_kernel, nf, nt), out_shape=jax.Sha...  199 us

profile of v1, /device:TPU:0, one launch (start us, length us, event | category | flops | bytes accessed | tf_op | source)
XLA Modules:
  0.0 202.4 jit_solution(3465341467013274694)
XLA Ops:
  0.0 199.3 %shard_map.91 = bf16[512,2048]{1,0:T(8,128)(2,1)} custom-call(bf16[512,2048]{1,0:T(8,128)(2,1)} %refs_0_.1, f32[2,2048]{1,0:T(2,128)} %refs_1_.1, f32[2,2048]{1,0:T(2,128)} %refs_2_.1, bf16[512,768]{1,0:T(8,128)(2,1)} %refs_3_.1, bf16[512,768]{1,0:T(8,128)(2,1)} %refs_4_.1, bf16[768,512]{1,0:T(8,128)(2,1)} %refs_5_.1, bf16[512,768]{1,0:T(8,128)(2,1)} %refs_6_.1, ...), custom_call_target="tpu_custom_call" | custom-call | tf_op jit(solution)/shard_map/pallas_call | solution.py:294
  199.3 3.2 %copy.11 = bf16[512,2048]{1,0:T(8,128)(2,1)} copy(bf16[512,2048]{1,0:T(8,128)(2,1)} %shard_map.91) | data formatting | bytes 4194304

commit v2 on v0

--- a/solution.py
+++ b/solution.py
@@ -1,7 +1,376 @@
+import functools
+
 import jax
 import jax.numpy as jnp
 from jax import lax
+from jax.experimental import pallas as pl
+from jax.experimental.pallas import tpu as pltpu
 from jax.sharding import PartitionSpec as P
+
+MESH = pl.DeviceIdType.MESH
+SCALE = 2.0**0.25
+F32 = jnp.float32
+BF16 = jnp.bfloat16
+
+
+def aligned(value, step):
+    return pl.multiple_of(value, step)
+
+
+def fused_kernel(nf, nt, *refs):
+    gains, shifts, tokens = refs[:3]
+    shards = refs[3:9]
+    out = refs[9]
+    full = refs[10:16]
+    stream, gate, hidden, part, middle, pair, ring = refs[16:23]
+    (z_recv, extra_recv, y_recv, line_sent, mate_sent, extra_sent, y_sent, own_done,
+     core_sent, core_recv, x_sent, x_recv, back_sent, back_recv,
+     swap_sent, swap_recv, hand_sent, hand_recv, tokens_done) = refs[23:]
+
+    g = lax.axis_index("grp")
+    f = lax.axis_index("fs")
+    t = lax.axis_index("tp")
+    other_g = 1 - g
+    chip, core = t // 2, t % 2
+    chips = nt // 2
+    peer = chip * 2 + (1 - core)
+    rows, width = tokens.shape
+    half = rows // 2
+    depth = width // nf
+
+    at_end = (f == 0) | (f == nf - 1)
+    inside = (f > 0) & (f < nf - 1)
+    low = f < nf // 2
+    mate = jnp.where(low, 1 - f, 2 * nf - 3 - f)
+    facing = nf - 1 - f
+    far = nf - 1 - mate
+    mine = pl.ds(aligned(core * half, half), half)
+    theirs = pl.ds(aligned((1 - core) * half, half), half)
+
+    def tell(**where):
+        pl.semaphore_signal(barrier, inc=1, device_id=where, device_id_type=MESH)
+
+    barrier = pltpu.get_barrier_semaphore()
+    tell(fs=mate)
+    pl.when(inside)(lambda: tell(fs=facing))
+    tell(grp=other_g)
+    tell(tp=peer)
+    for step in range(1, chips):
+        tell(tp=lax.rem(chip + step, chips) * 2 + core)
+    pl.semaphore_wait(barrier, jnp.where(inside, 1, 0) + 2 + chips)
+
+    def remote(src, dst, sent, received, **where):
+        return pltpu.make_async_remote_copy(
+            src, dst, sent, received, device_id=where, device_id_type=MESH)
+
+    def shard_part(a, which):
+        size = shards[a].shape[0] // 2
+        return shards[a].at[pl.ds(aligned(which * size, size), size), :]
+
+    def slot(a, s, which):
+        if a % 3 == 2:
+            size = full[a].shape[1] // 2
+            return full[a].at[s, pl.ds(aligned(which * size, size), size), :]
+        size = depth // 2
+        return full[a].at[pl.ds(aligned(s * depth + which * size, size), size), :]
+
+    def whole_slot(a, s):
+        if a % 3 == 2:
+            return full[a].at[s]
+        return full[a].at[pl.ds(aligned(s * depth, depth), depth), :]
+
+    def columns(s):
+        return pl.ds(aligned(s * depth, depth), depth)
+
+    both_parts = range(1, 6)
+
+    def own(a):
+        return pltpu.make_async_copy(shards[a], whole_slot(a, f), own_done.at[a])
+
+    def from_end(a, s):
+        return remote(shard_part(a, g), slot(a, s, g), mate_sent.at[a], z_recv.at[a, s], fs=mate)
+
+    def extra(a, s):
+        return remote(
+            shard_part(a, other_g), slot(a, s, other_g), extra_sent.at[a], extra_recv.at[a],
+            fs=mate)
+
+    def along(a, s, src):
+        return remote(src, slot(a, s, g), line_sent.at[a, s], z_recv.at[a, s], fs=facing)
+
+    def across(a, s, which):
+        return remote(
+            slot(a, s, which), slot(a, s, which), y_sent.at[a, s], y_recv.at[a, s], grp=other_g)
+
+    def hand_tokens():
+        return remote(
+            tokens.at[mine, :], stream.at[1, mine, :], hand_sent.at[0], hand_recv.at[0], fs=mate)
+
+    def share_tokens(where):
+        return remote(
+            stream.at[1, where, :], stream.at[1, where, :], hand_sent.at[1], hand_recv.at[1],
+            tp=peer)
+
+    def hand_middle():
+        return remote(
+            middle.at[1, mine, :], middle.at[0, mine, :], hand_sent.at[2], hand_recv.at[2],
+            fs=mate)
+
+    def core_copy(layer, s):
+        return remote(
+            part.at[layer, :, theirs, columns(s)], pair.at[layer, :, :, columns(s)],
+            core_sent.at[layer, s], core_recv.at[layer, s], tp=peer)
+
+    def x_view(layer, s, source):
+        if layer == 0:
+            return ring.at[0, source, :, :, columns(s)]
+        return ring.at[1, source, 0, :, columns(s)]
+
+    def x_copy(layer, s, source, target):
+        return remote(
+            x_view(layer, s, source), x_view(layer, s, source),
+            x_sent.at[layer, s, target], x_recv.at[layer, s, source], tp=target * 2 + core)
+
+    def back(s):
+        return remote(
+            ring.at[1, chip, 1, :, columns(s)], ring.at[1, chip, 0, :, columns(s)],
+            back_sent.at[s], back_recv.at[s], fs=mate)
+
+    def swap(layer, where):
+        view = middle.at[:, where, :] if layer == 0 else out.at[where, :]
+        return remote(view, view, swap_sent.at[layer], swap_recv.at[layer], tp=peer)
+
+    def x_start(layer, s):
+        for step in range(1, chips):
+            x_copy(layer, s, chip, lax.rem(chip + step, chips)).start()
+
+    def x_arrived(layer, s):
+        for step in range(1, chips):
+            source = lax.rem(chip + step, chips)
+            x_copy(layer, s, source, source).wait_recv()
+
+    def x_left(layer, s):
+        for step in range(1, chips):
+            x_copy(layer, s, chip, lax.rem(chip + step, chips)).wait_send()
+
+    tile = 256 if gate.shape[2] % 256 == 0 else gate.shape[2]
+    tiles = gate.shape[2] // tile
+
+    def project_gate(a, source):
+        @pl.loop(0, 2 * tiles)
+        def _(i):
+            block, cols = i // tiles, pl.ds(aligned((i % tiles) * tile, tile), tile)
+            gate[block, :, cols] = jnp.dot(
+                source[block], full[a][:, cols], preferred_element_type=F32)
+
+    def project_up(a, source):
+        @pl.loop(0, 2 * tiles)
+        def _(i):
+            block, cols = i // tiles, pl.ds(aligned((i % tiles) * tile, tile), tile)
+            up = jnp.dot(source[block], full[a][:, cols], preferred_element_type=F32)
+            hidden[block, :, cols] = (jax.nn.silu(gate[block, :, cols]) * up).astype(BF16)
+
+    def partial(layer, s):
+        @pl.loop(0, 2)
+        def _(block):
+            part[layer, block, :, columns(s)] = jnp.dot(
+                hidden[block], full[3 * layer + 2][s], preferred_element_type=F32).astype(BF16)
+        core_copy(layer, s).start()
+
+    def pair_sum(layer, s):
+        core_copy(layer, s).wait_recv()
+        for block in (1, 0):
+            ring[layer, chip, block, :, columns(s)] = (
+                part[layer, block, mine, columns(s)].astype(F32)
+                + pair[layer, block, :, columns(s)].astype(F32)
+            ).astype(BF16)
+            if layer == 1 and block == 1:
+                back(s).start()
+        x_start(layer, s)
+
+    def norm(layer, block, source, target):
+        band = 32
+
+        @pl.loop(0, half // band)
+        def _(i):
+            here = pl.ds(aligned(i * band, band), band)
+            there = pl.ds(aligned(core * half + i * band, band), band)
+            total = ring[layer, 0, block, here, :].astype(F32)
+            for c in range(1, chips):
+                total = total + ring[layer, c, block, here, :].astype(F32)
+            branch = total.astype(BF16).astype(F32)
+            v = SCALE * source[block, there, :].astype(F32) + 0.5 * branch
+            v = v - jnp.mean(v, axis=-1, keepdims=True)
+            spread = jnp.mean(v * v, axis=-1, keepdims=True)
+            normed = v * lax.rsqrt(spread + 1e-05)
+            done = (normed * gains[layer:layer + 1, :] + shifts[layer:layer + 1, :]).astype(BF16)
+            if layer == 0:
+                target[block, there, :] = done
+            else:
+                target[there, :] = done
+
+    def finish():
+        norm(1, 0, middle, out)
+        swap(1, mine).start()
+        swap(1, theirs).wait_recv()
+        swap(1, mine).wait_send()
+
+    @pl.when(at_end)
+    def _():
+        from_end(0, f).start()
+        hand_tokens().start()
+        for a in range(1, 6):
+            from_end(a, f).start()
+            if a in both_parts:
+                extra(a, f).start()
+        hand_middle().wait_recv()
+        for s in (mate, f, nf - 1 - mate, nf - 1 - f):
+            back(s).wait_recv()
+            x_start(1, s)
+        pl.loop(0, nf)(lambda s: x_arrived(1, s))
+        finish()
+        hand_tokens().wait_send()
+        for a in range(6):
+            from_end(a, f).wait_send()
+            if a in both_parts:
+                extra(a, f).wait_send()
+        pl.loop(0, nf)(lambda s: x_left(1, s))
+
+    def mate_part(a):
+        from_end(a, mate).wait_recv()
+        along(a, mate, slot(a, mate, g)).start()
+        if a not in both_parts:
+            across(a, mate, g).start()
+
+    def line_part(a, s):
+        along(a, s, slot(a, s, g)).wait_recv()
+        across(a, s, g).start()
+
+    def mate_whole(a):
+        if a in both_parts:
+            extra(a, mate).wait_recv()
+        else:
+            across(a, mate, other_g).wait_recv()
+
+    def crossed(a, s):
+        across(a, s, other_g).wait_recv()
+
+    def arrived(a):
+        own(a).wait()
+        mate_whole(a)
+        crossed(a, facing)
+        crossed(a, far)
+
+    @pl.when(inside)
+    def _():
+        along(0, f, shard_part(0, g)).start()
+        own_tokens = pltpu.make_async_copy(tokens, stream.at[0], tokens_done)
+        own_tokens.start()
+        for a in range(6):
+            own(a).start()
+
+        for a in range(6):
+            if a < 5:
+                along(a + 1, f, shard_part(a + 1, g)).start()
+            if a == 0:
+                line_part(a, facing)
+                mate_part(a)
+            else:
+                mate_part(a)
+                line_part(a, facing)
+            if a == 1:
+                hand_tokens().wait_recv()
+                share_tokens(mine).start()
+                own_tokens.wait()
+                share_tokens(theirs).wait_recv()
+                arrived(0)
+                project_gate(0, stream)
+            if a == 2:
+                arrived(1)
+                project_up(1, stream)
+            if a == 3:
+                arrived(2)
+                pl.loop(0, nf)(lambda s: partial(0, s))
+                pl.loop(0, nf)(lambda s: pair_sum(0, s))
+            line_part(a, far)
+
+        pl.loop(0, nf)(lambda s: x_arrived(0, s))
+        norm(0, 0, stream, middle)
+        norm(0, 1, stream, middle)
+        swap(0, mine).start()
+        hand_middle().start()
+        swap(0, theirs).wait_recv()
+        arrived(3)
+        project_gate(3, middle)
+        arrived(4)
+        project_up(4, middle)
+        own(5).wait()
+        partial(1, f)
+        mate_whole(5)
+        partial(1, mate)
+        pair_sum(1, f)
+        crossed(5, facing)
+        partial(1, facing)
+        pair_sum(1, mate)
+        crossed(5, far)
+        partial(1, far)
+        pair_sum(1, facing)
+        pair_sum(1, far)
+        pl.loop(0, nf)(lambda s: x_arrived(1, s))
+        finish()
+
+        share_tokens(mine).wait_send()
+        hand_middle().wait_send()
+        swap(0, mine).wait_send()
+        for a in range(6):
+            along(a, f, slot(a, f, g)).wait_send()
+            along(a, mate, slot(a, mate, g)).wait_send()
+            across(a, facing, g).wait_send()
+            across(a, far, g).wait_send()
+            if a not in both_parts:
+                across(a, mate, g).wait_send()
+
+        @pl.loop(0, nf)
+        def _(s):
+            back(s).wait_send()
+            for layer in range(2):
+                core_copy(layer, s).wait_send()
+                x_left(layer, s)
+
+
+def fused(nf, nt, tokens, gains, shifts, *weights):
+    rows, width = tokens.shape
+    units = weights[0].shape[1]
+    depth = width // nf
+    half = rows // 2
+    side = pltpu.VMEM((width, units), BF16)
+    down = pltpu.VMEM((nf, units, depth), BF16)
+    dma = pltpu.SemaphoreType.DMA
+    chips = nt // 2
+    return pl.pallas_call(
+        functools.partial(fused_kernel, nf, nt),
+        out_shape=jax.ShapeDtypeStruct((rows, width), BF16),
+        in_specs=[pl.BlockSpec(memory_space=pltpu.VMEM)] * 2
+        + [pl.BlockSpec(memory_space=pl.ANY)] * 7,
+        out_specs=pl.BlockSpec(memory_space=pltpu.VMEM),
+        scratch_shapes=[
+            side, side, down, side, side, down,
+            pltpu.VMEM((2, rows, width), BF16),
+            pltpu.VMEM((2, rows, units), F32),
+            pltpu.VMEM((2, rows, units), BF16),
+            pltpu.VMEM((2, 2, rows, width), BF16),
+            pltpu.VMEM((2, rows, width), BF16),
+            pltpu.VMEM((2, 2, half, width), BF16),
+            pltpu.VMEM((2, chips, 2, half, width), BF16),
+            dma((6, nf)), dma((6,)), dma((6, nf)), dma((6, nf)), dma((6,)), dma((6,)),
+            dma((6, nf)), dma((6,)),
+            dma((2, nf)), dma((2, nf)), dma((2, nf, chips)), dma((2, nf, chips)),
+            dma((nf,)), dma((nf,)),
+            dma((2,)), dma((2,)), dma((3,)), dma((3,)), dma,
+        ],
+        compiler_params=pltpu.CompilerParams(
+            collective_id=0, has_side_effects=True, vmem_limit_bytes=63 * 1024 * 1024),
+    )(gains, shifts, tokens, *weights)
 
 
 def post_norm(values, gain, shift):
@@ -52,7 +421,22 @@
     return half_step(middle, gate_second, up_second, down_second, norm_gain[1], norm_shift[1])
 
 
+def fits(mesh, args):
+    tokens, gate_first = args[0], args[3]
+    nf, nt = mesh.shape["fs"], mesh.shape["tp"]
+    depth, units = gate_first.shape
+    return (
+        mesh.shape["grp"] == 2 and nt % 2 == 0 and nf == 4
+        and depth % 128 == 0 and units % 128 == 0 and tokens.shape[0] % 64 == 0
+    )
+
+
 def solution(mesh):
+    def either(*args):
+        if fits(mesh, args):
+            return fused(mesh.shape["fs"], mesh.shape["tp"], *args)
+        return local(*args)
+
     placed = (
         P(("grp", "fs"), None),
         P(),
@@ -65,5 +449,5 @@
         P("tp", "fs"),
     )
     return jax.shard_map(
-        local, mesh=mesh, in_specs=placed, out_specs=P(("grp", "fs"), None), check_vma=False
+        either, mesh=mesh, in_specs=placed, out_specs=P(("grp", "fs"), None), check_vma=False
     )

time: 520 us -> 203 us (0.39)
  waiting for transfers between devices: 467 us -> 0 us
  Pallas kernels: 0 us -> 200 us
  matrix products: 26.1 us -> 0 us
  between operations: 13.6 us -> 0.01 us
  other arithmetic: 11.6 us -> 0 us
    all_gather x6 -> x0, waiting for transfers between devices: 365 us -> none  [the longest x2 127 us: half_step(): lax.all_gather(up_w, 'fs', axis=0, tiled=True)]
    pallas_call x0 -> x1, Pallas kernels: none -> 200 us  [fused(): pl.pallas_call(functools.partial(fused_kernel, nf, nt), out_shape=jax.Sha...]
    psum x2 -> x0, waiting for transfers between devices: 98.1 us -> none  [half_step(): lax.psum(partial_value, 'tp').astype(jnp.float32).astype(jnp.bfloat16)]
    dot_general x4 -> x0, matrix products: 26.1 us -> none  [the longest x2 14.9 us: half_step(): both = jnp.dot(stream, joined, preferred_element_type=jnp.float32)]
    reduce_sum x4 -> x0, other arithmetic: 7.58 us -> none  [the longest x2 5.25 us: post_norm(): mean = jnp.mean(values, axis=-1, keepdims=True)]
  transfers between devices with their start and end apart: 8 -> 0, of which waited for: 8 -> 0; matrix products, arithmetic and copies ran while one was open for 4% -> 0% of each run, Pallas kernels for 0% -> 0%
where the time goes in v2:
time: 203 us
  Pallas kernels  200 us (99%)
  local copies, waits for them, and re-layouts  3.16 us (2%)
    pallas_call x1, Pallas kernels, fused(): pl.pallas_call(functools.partial(fused_kernel, nf, nt), out_shape=jax.Sha...  200 us

profile of v2, /device:TPU:0, one launch (start us, length us, event | category | flops | bytes accessed | tf_op | source)
XLA Modules:
  0.0 202.9 jit_solution(8024021805115617377)
XLA Ops:
  0.0 199.7 %shard_map.91 = bf16[512,2048]{1,0:T(8,128)(2,1)} custom-call(f32[2,2048]{1,0:T(2,128)} %refs_0_.1, f32[2,2048]{1,0:T(2,128)} %refs_1_.1, bf16[512,2048]{1,0:T(8,128)(2,1)} %refs_2_.1, bf16[512,768]{1,0:T(8,128)(2,1)} %refs_3_.1, bf16[512,768]{1,0:T(8,128)(2,1)} %refs_4_.1, bf16[768,512]{1,0:T(8,128)(2,1)} %refs_5_.1, bf16[512,768]{1,0:T(8,128)(2,1)} %refs_6_.1, ...), custom_call_target="tpu_custom_call" | custom-call | tf_op jit(solution)/shard_map/pallas_call | solution.py:350
  199.8 3.2 %copy.11 = bf16[512,2048]{1,0:T(8,128)(2,1)} copy(bf16[512,2048]{1,0:T(8,128)(2,1)} %shard_map.91) | data formatting | bytes 4194304

commit v3 on v2

--- a/solution.py
+++ b/solution.py
@@ -25,7 +25,7 @@
     stream, gate, hidden, part, middle, pair, ring = refs[16:23]
     (z_recv, extra_recv, y_recv, line_sent, mate_sent, extra_sent, y_sent, own_done,
      core_sent, core_recv, x_sent, x_recv, back_sent, back_recv,
-     swap_sent, swap_recv, hand_sent, hand_recv, tokens_done) = refs[23:]
+     swap_sent, swap_recv, hand_sent, hand_recv, tokens_done, spread_sent, spread_recv) = refs[23:]
 
     g = lax.axis_index("grp")
     f = lax.axis_index("fs")
@@ -82,7 +82,7 @@
     def columns(s):
         return pl.ds(aligned(s * depth, depth), depth)
 
-    both_parts = range(1, 6)
+    both_parts = range(6)
 
     def own(a):
         return pltpu.make_async_copy(shards[a], whole_slot(a, f), own_done.at[a])
@@ -104,7 +104,17 @@
 
     def hand_tokens():
         return remote(
-            tokens.at[mine, :], stream.at[1, mine, :], hand_sent.at[0], hand_recv.at[0], fs=mate)
+            tokens.at[piece(chip), :], stream.at[1, piece(chip), :],
+            hand_sent.at[0], hand_recv.at[0], fs=mate)
+
+    def piece(which):
+        size = half // chips
+        return pl.ds(aligned(core * half + which * size, size), size)
+
+    def spread_tokens(source, target):
+        return remote(
+            stream.at[1, piece(source), :], stream.at[1, piece(source), :],
+            spread_sent.at[target], spread_recv.at[source], tp=target * 2 + core)
 
     def share_tokens(where):
         return remote(
@@ -217,23 +227,24 @@
 
     @pl.when(at_end)
     def _():
-        from_end(0, f).start()
-        hand_tokens().start()
+        queue = [from_end(0, f), hand_tokens()]
         for a in range(1, 6):
-            from_end(a, f).start()
-            if a in both_parts:
-                extra(a, f).start()
+            queue.append(from_end(a, f))
+            if a - 1 in both_parts:
+                queue.append(extra(a - 1, f))
+        queue.append(extra(5, f))
+        for k, copy in enumerate(queue):
+            if k >= 2:
+                queue[k - 2].wait_send()
+            copy.start()
+        queue[-2].wait_send()
+        queue[-1].wait_send()
         hand_middle().wait_recv()
         for s in (mate, f, nf - 1 - mate, nf - 1 - f):
             back(s).wait_recv()
             x_start(1, s)
         pl.loop(0, nf)(lambda s: x_arrived(1, s))
         finish()
-        hand_tokens().wait_send()
-        for a in range(6):
-            from_end(a, f).wait_send()
-            if a in both_parts:
-                extra(a, f).wait_send()
         pl.loop(0, nf)(lambda s: x_left(1, s))
 
     def mate_part(a):
@@ -264,14 +275,15 @@
     @pl.when(inside)
     def _():
         along(0, f, shard_part(0, g)).start()
+        along(1, f, shard_part(1, g)).start()
         own_tokens = pltpu.make_async_copy(tokens, stream.at[0], tokens_done)
         own_tokens.start()
         for a in range(6):
             own(a).start()
 
         for a in range(6):
-            if a < 5:
-                along(a + 1, f, shard_part(a + 1, g)).start()
+            if a < 4:
+                along(a + 2, f, shard_part(a + 2, g)).start()
             if a == 0:
                 line_part(a, facing)
                 mate_part(a)
@@ -279,7 +291,12 @@
                 mate_part(a)
                 line_part(a, facing)
             if a == 1:
+                others = [lax.rem(chip + step, chips) for step in range(1, chips)]
                 hand_tokens().wait_recv()
+                for c in others:
+                    spread_tokens(chip, c).start()
+                for c in others:
+                    spread_tokens(c, c).wait_recv()
                 share_tokens(mine).start()
                 own_tokens.wait()
                 share_tokens(theirs).wait_recv()
@@ -288,11 +305,21 @@
             if a == 2:
                 arrived(1)
                 project_up(1, stream)
+                own(2).wait()
+                partial(0, f)
+                mate_whole(2)
+                partial(0, mate)
+                pair_sum(0, f)
             if a == 3:
-                arrived(2)
-                pl.loop(0, nf)(lambda s: partial(0, s))
-                pl.loop(0, nf)(lambda s: pair_sum(0, s))
+                crossed(2, facing)
+                partial(0, facing)
+                pair_sum(0, mate)
             line_part(a, far)
+            if a == 3:
+                crossed(2, far)
+                partial(0, far)
+                pair_sum(0, facing)
+                pair_sum(0, far)
 
         pl.loop(0, nf)(lambda s: x_arrived(0, s))
         norm(0, 0, stream, middle)
@@ -320,6 +347,8 @@
         finish()
 
         share_tokens(mine).wait_send()
+        for step in range(1, chips):
+            spread_tokens(chip, lax.rem(chip + step, chips)).wait_send()
         hand_middle().wait_send()
         swap(0, mine).wait_send()
         for a in range(6):
@@ -367,6 +396,7 @@
             dma((2, nf)), dma((2, nf)), dma((2, nf, chips)), dma((2, nf, chips)),
             dma((nf,)), dma((nf,)),
             dma((2,)), dma((2,)), dma((3,)), dma((3,)), dma,
+            dma((chips,)), dma((chips,)),
         ],
         compiler_params=pltpu.CompilerParams(
             collective_id=0, has_side_effects=True, vmem_limit_bytes=63 * 1024 * 1024),

time: 203 us -> 193 us (0.951)
  Pallas kernels: 200 us -> 189 us
    pallas_call x1, Pallas kernels: 200 us -> 189 us  [fused(): pl.pallas_call(functools.partial(fused_kernel, nf, nt), out_shape=jax.Sha...]
where the time goes in v3:
time: 193 us
  Pallas kernels  189 us (98%)
  local copies, waits for them, and re-layouts  3.16 us (2%)
    pallas_call x1, Pallas kernels, fused(): pl.pallas_call(functools.partial(fused_kernel, nf, nt), out_shape=jax.Sha...  189 us

profile of v3, /device:TPU:0, one launch (start us, length us, event | category | flops | bytes accessed | tf_op | source)
XLA Modules:
  0.0 192.7 jit_solution(12372472621835148341)
XLA Ops:
  0.0 189.5 %shard_map.91 = bf16[512,2048]{1,0:T(8,128)(2,1)} custom-call(f32[2,2048]{1,0:T(2,128)} %refs_0_.1, f32[2,2048]{1,0:T(2,128)} %refs_1_.1, bf16[512,2048]{1,0:T(8,128)(2,1)} %refs_2_.1, bf16[512,768]{1,0:T(8,128)(2,1)} %refs_3_.1, bf16[512,768]{1,0:T(8,128)(2,1)} %refs_4_.1, bf16[768,512]{1,0:T(8,128)(2,1)} %refs_5_.1, bf16[512,768]{1,0:T(8,128)(2,1)} %refs_6_.1, ...), custom_call_target="tpu_custom_call" | custom-call | tf_op jit(solution)/shard_map/pallas_call | solution.py:379
  189.5 3.2 %copy.11 = bf16[512,2048]{1,0:T(8,128)(2,1)} copy(bf16[512,2048]{1,0:T(8,128)(2,1)} %shard_map.91) | data formatting | bytes 4194304
